TPU v7x, 32 devices: a whole 2x2x4 slice. The times are simulated.
32 devices in a mesh: grp: 2 (over y), fs: 4 (over z), tp: 4 (over x, core).
Axes of the slice: x: 2, y: 2, z: 4, core: 2. Of those that a mesh axis runs over, the one named last changes fastest.
Arguments:
- tokens: bfloat16 [2048, 2048], P(('grp', 'fs', 'tp')), parts along dimension 0, may hold values from -30 to 30
- gate_master: float32 [2048, 2752], P('fs', 'tp'), may hold values from -0.125 to 0.125
- up_master: float32 [2048, 2752], P('fs', 'tp'), may hold values from -0.125 to 0.125
- down_master: float32 [2048, 2752], P('fs', 'tp'), may hold values from -0.4375 to 0.4375
- norm_gain: float32 [2048], replicated, may hold values from 0.1 to 1.9
- post_gain: float32 [2048], replicated, may hold values from 0.1 to 1.9
- post_bias: float32 [2048], replicated, may hold values from -3 to 3
Outputs:
- gate_ready: bfloat16 [4096, 2752], P('grp', 'tp'), parts along dimension 0
- up_ready: bfloat16 [4096, 2752], P('grp', 'tp'), parts along dimension 0
- down_ready: bfloat16 [4096, 2752], P('grp', 'tp'), parts along dimension 0
- result: bfloat16 [2048, 2048], P(('grp', 'fs', 'tp')), parts along dimension 0
There are 2 independent parts, one for each index of `grp`. A program takes and returns all parts, laid end to end along the dimension named above; an argument that names none is the same for every part. Nothing has to cross between parts.
All inputs are finite; a program needn't handle non-finite values.
Results may differ from a plain program's by a relative error of at most 0.009.
Values may be sent and summed in bfloat16 or wider, within the bound.
A program may use at most 64 MiB of HBM per device.

v0:
```python
import jax
import jax.numpy as jnp
from jax import lax
from jax.sharding import PartitionSpec as P


def finish(wide, branch, post_gain, post_bias):
    mixed = jnp.sqrt(jnp.float32(2.0)) * wide + 0.5 * branch
    center = jnp.mean(mixed, axis=-1, keepdims=True)
    spread = jnp.mean(jnp.square(mixed - center), axis=-1, keepdims=True)
    return ((mixed - center) * lax.rsqrt(spread + 1e-05) * post_gain + post_bias).astype(
        jnp.bfloat16
    )


def local(tokens, gate_master, up_master, down_master, norm_gain, post_gain, post_bias):
    row_count = gate_master.shape[0]
    first_row = lax.axis_index("fs") * row_count
    gain_rows = lax.dynamic_slice_in_dim(norm_gain, first_row, row_count, 0)
    gate_piece = (gain_rows[:, None] * gate_master).astype(jnp.bfloat16)
    up_piece = (gain_rows[:, None] * up_master).astype(jnp.bfloat16)
    down_piece = down_master.astype(jnp.bfloat16)
    gate_ready, up_ready, down_ready = (
        lax.all_gather(gate_piece, "fs", axis=0, tiled=True),
        lax.all_gather(up_piece, "fs", axis=0, tiled=True),
        lax.all_gather(down_piece, "fs", axis=0, tiled=True),
    )
    wide = tokens.astype(jnp.float32)
    normed = (wide * lax.rsqrt(jnp.mean(wide * wide, axis=-1, keepdims=True) + 1e-06)).astype(
        jnp.bfloat16
    )
    piece = lax.all_gather(normed, "tp", axis=0, tiled=True)
    gate = jnp.dot(piece, gate_ready, preferred_element_type=jnp.float32)
    upward = jnp.dot(piece, up_ready, preferred_element_type=jnp.float32)
    hidden = (jax.nn.silu(gate) * upward).astype(jnp.bfloat16)
    branch = lax.psum_scatter(
        lax.dot_general(
            hidden, down_ready, (((1,), (1,)), ((), ())), preferred_element_type=jnp.float32
        ).astype(jnp.bfloat16),
        "tp",
        scatter_dimension=0,
        tiled=True,
    ).astype(jnp.float32)
    result = finish(wide, branch, post_gain, post_bias)
    return (gate_ready, up_ready, down_ready, result)


def solution(mesh):
    return jax.shard_map(
        local,
        mesh=mesh,
        in_specs=(
            P(("grp", "fs", "tp"), None),
            P("fs", "tp"),
            P("fs", "tp"),
            P("fs", "tp"),
            P(),
            P(),
            P(),
        ),
        out_specs=(P("grp", "tp"), P("grp", "tp"), P("grp", "tp"), P(("grp", "fs", "tp"), None)),
        check_vma=False,
    )
```

profile of v0, /device:TPU:0, one launch (start us, length us, event | category | flops | bytes accessed | tf_op | source)
XLA Modules:
  0.0 256.1 jit_solution(3088402425451007015)
XLA Ops:
  7.2 0.0 all-gather.11.cloned.1.call-start
  7.2 1.1 fusion.2
  8.3 1.8 fusion.3
  10.1 0.0 all-gather.11.cloned.1.call-update
  10.1 0.0 all-gather.5.cloned.1.call-start
  10.2 0.8 dynamic_slice.3
  10.9 0.0 copy-start.4
  10.9 3.3 %multiply_convert_fusion = (bf16[512,688]{0,1:T(8,128)(2,1)}, bf16[512,688]{0,1:T(8,128)(2,1)}) fusion(f32[512,688]{0,1:T(8,128)} %param.9, f32[512]{0:T(512)S(1)} %dynamic_slice.3, f32[512,688]{0,1:T(8,128)} %param.8), kind=kLoop, calls=%fused_computation.1 | loop fusion | flops 1409024 | bytes 4229120 | tf_op jit(solution)/shard_map/convert_element_type | solution.py:21
  14.3 0.0 all-gather.5.cloned.1.call-update
  14.3 0.0 all-gather.7.cloned.1.call-start
  14.4 0.7 all-gather.7.cloned.1.call-update
  15.1 0.0 all-gather.9.cloned.1.call-start
  15.1 0.0 copy-done.4
  15.1 0.9 convert_element_type.29
  16.1 0.0 all-gather.9.cloned.1.call-update
  16.1 0.0 reduce-scatter.2.cloned.1.call-start
  16.1 13.6 %all-gather.11.cloned.1.call-done = bf16[256,2048]{1,0:T(8,128)(2,1)} async-done(((bf16[64,2048]{1,0:T(8,128)(2,1)}), bf16[256,2048]{1,0:T(8,128)(2,1)}) %all-gather.11.cloned.1.call-update) | async-done | bytes 1048592 | tf_op jit(solution)/shard_map/all_gather | solution.py:32
  29.7 0.0 copy-start.7
  29.7 60.2 %all-gather.5.cloned.1.call-done = bf16[2048,688]{0,1:T(8,128)(2,1)} async-done(((bf16[512,688]{0,1:T(8,128)(2,1)}), bf16[2048,688]{0,1:T(8,128)(2,1)}) %all-gather.5.cloned.1.call-update) | async-done | bytes 2818064 | tf_op jit(solution)/shard_map/all_gather | solution.py:24
  89.9 3.0 %fusion.7 = f32[256,688]{0,1:T(8,128)S(1)} fusion(bf16[256,2048]{1,0:T(8,128)(2,1)} %all-gather.11.cloned.1.call-done, bf16[2048,688]{0,1:T(8,128)(2,1)} %all-gather.5.cloned.1.call-done), kind=kOutput, calls=%fused_computation.19 | convolution fusion | flops 721420288 | bytes 4571136 | tf_op jit(solution)/shard_map/dot_general | solution.py:33
  93.0 0.0 copy-start
  93.0 0.0 copy-start.5
  93.0 0.0 copy-start.6
  93.0 55.8 %all-gather.7.cloned.1.call-done = bf16[2048,688]{0,1:T(8,128)(2,1)} async-done(((bf16[512,688]{0,1:T(8,128)(2,1)}), bf16[2048,688]{0,1:T(8,128)(2,1)}) %all-gather.7.cloned.1.call-update) | async-done | bytes 2818064 | tf_op jit(solution)/shard_map/all_gather | solution.py:25
  148.8 58.8 %all-gather.9.cloned.1.call-done = bf16[2048,688]{0,1:T(8,128)(2,1)} async-done(((bf16[512,688]{0,1:T(8,128)(2,1)}), bf16[2048,688]{0,1:T(8,128)(2,1)}) %all-gather.9.cloned.1.call-update) | async-done | bytes 2818064 | tf_op jit(solution)/shard_map/all_gather | solution.py:26
  207.6 0.0 copy-done.7
  207.6 6.9 %convolution_convert_fusion = bf16[256,2048]{1,0:T(8,128)(2,1)} fusion(bf16[2048,688]{0,1:T(8,128)(2,1)} %all-gather.9.cloned.1.call-done, bf16[256,2048]{1,0:T(8,128)(2,1)S(1)} %copy-done.7, bf16[2048,688]{0,1:T(8,128)(2,1)} %all-gather.7.cloned.1.call-done, f32[256,688]{0,1:T(8,128)S(1)} %fusion.7), kind=kOutput, calls=%fused_computation | convolution fusion | flops 1444421632 | bytes 8437760 | tf_op jit(solution)/shard_map/dot_general | solution.py:37
  214.5 0.0 copy-start.1
  214.5 0.0 reduce-scatter.2.cloned.1.call-update
  214.5 23.7 %reduce-scatter.2.cloned.1.call-done = bf16[64,2048]{1,0:T(8,128)(2,1)} async-done(((bf16[256,2048]{1,0:T(8,128)(2,1)}), bf16[64,2048]{1,0:T(8,128)(2,1)}) %reduce-scatter.2.cloned.1.call-update) | async-done | bytes 262160 | tf_op jit(solution)/shard_map/reduce_scatter | solution.py:36
  238.2 0.0 copy-done
  238.2 1.2 fusion.5
  239.3 1.2 multiply_reduce_fusion
  240.5 0.0 copy-done.5
  240.6 0.0 copy-done.6
  240.6 1.8 add_convert_fusion
  242.4 0.0 copy-done.1
  242.4 0.0 copy-start.2
  242.4 1.6 copy.14
  244.0 1.3 copy-done.2
  245.2 0.0 copy-start.3
  245.2 1.6 copy.15
  246.8 1.3 copy-done.3
  248.0 1.6 copy.16
  (3 shorter events, 0.0 us)
Async XLA Ops:
  7.2 22.5 %all-gather.11.cloned.1.call-start = ((), (), s32[]{:S(2)}) async-start(), calls=%async_computation.4 | async-start | bytes 1310720 | tf_op jit(solution)/shard_map/all_gather | solution.py:32
  10.1 79.8 %all-gather.5.cloned.1.call-start = ((), (), s32[]{:S(2)}) async-start(), calls=%async_computation.1 | async-start | bytes 3522560 | tf_op jit(solution)/shard_map/all_gather | solution.py:24
  10.9 4.2 %copy-start.4 = (f32[512,688]{0,1:T(8,128)S(1)}, f32[512,688]{0,1:T(8,128)}, u32[]{:S(2)}) copy-start(f32[512,688]{0,1:T(8,128)} %param.10) | copy-start | bytes 4227076
  14.3 134.5 %all-gather.7.cloned.1.call-start = ((), (), s32[]{:S(2)}) async-start(), calls=%async_computation.2 | async-start | bytes 3522560 | tf_op jit(solution)/shard_map/all_gather | solution.py:25
  15.1 192.5 %all-gather.9.cloned.1.call-start = ((), (), s32[]{:S(2)}) async-start(), calls=%async_computation.3 | async-start | bytes 3522560 | tf_op jit(solution)/shard_map/all_gather | solution.py:26
  16.1 222.1 %reduce-scatter.2.cloned.1.call-start = ((), (), s32[]{:S(2)}) async-start(), calls=%async_computation.5 | async-start | bytes 1310720 | tf_op jit(solution)/shard_map/reduce_scatter | solution.py:36
  29.7 177.9 %copy-start.7 = (bf16[256,2048]{1,0:T(8,128)(2,1)S(1)}, bf16[256,2048]{1,0:T(8,128)(2,1)}, u32[]{:S(2)}) copy-start(bf16[256,2048]{1,0:T(8,128)(2,1)} %all-gather.11.cloned.1.call-done) | copy-start | bytes 3145732
  93.0 145.2 %copy-start = (bf16[64,2048]{1,0:T(8,128)(2,1)S(1)}, bf16[64,2048]{1,0:T(8,128)(2,1)}, u32[]{:S(2)}) copy-start(bf16[64,2048]{1,0:T(8,128)(2,1)} %param.7) | copy-start | bytes 786436
  93.0 147.6 %copy-start.5 = (f32[2048]{0:T(1024)S(1)}, f32[2048]{0:T(1024)}, u32[]{:S(2)}) copy-start(f32[2048]{0:T(1024)} %param.13) | copy-start | bytes 24580
  93.0 147.6 %copy-start.6 = (f32[2048]{0:T(1024)S(1)}, f32[2048]{0:T(1024)}, u32[]{:S(2)}) copy-start(f32[2048]{0:T(1024)} %param.12) | copy-start | bytes 24580
  214.5 27.9 %copy-start.1 = (bf16[2048,688]{0,1:T(8,128)(2,1)S(1)}, bf16[2048,688]{0,1:T(8,128)(2,1)}, u32[]{:S(2)}) copy-start(bf16[2048,688]{0,1:T(8,128)(2,1)} %all-gather.5.cloned.1.call-done) | copy-start | bytes 8454148
  242.4 2.8 %copy-start.2 = (bf16[2048,688]{0,1:T(8,128)(2,1)S(1)}, bf16[2048,688]{0,1:T(8,128)(2,1)}, u32[]{:S(2)}) copy-start(bf16[2048,688]{0,1:T(8,128)(2,1)} %all-gather.7.cloned.1.call-done) | copy-start | bytes 8454148
  245.2 2.8 %copy-start.3 = (bf16[2048,688]{0,1:T(8,128)(2,1)S(1)}, bf16[2048,688]{0,1:T(8,128)(2,1)}, u32[]{:S(2)}) copy-start(bf16[2048,688]{0,1:T(8,128)(2,1)} %all-gather.9.cloned.1.call-done) | copy-start | bytes 8454148
Sparse Core Ops, SparseCore 0:
  10.2 19.4 all-gather.10
  31.8 58.0 all-gather.4
  92.1 56.7 all-gather.6
  150.8 56.7 all-gather.8
  214.6 23.4 reduce-scatter.1
where the time goes:
time: 257 us; the launch traced here: 256 us
  waiting for transfers between devices  213 us (83%)
  between operations  13.9 us (5%)
  other arithmetic  11.4 us (4%)
  matrix products  9.93 us (4%)
  local copies, waits for them, and re-layouts  7.97 us (3%)
    all_gather x1, waiting for transfers between devices, local(): lax.all_gather(gate_piece, 'fs', axis=0, tiled=True)  60.2 us
    all_gather x1, waiting for transfers between devices, local(): lax.all_gather(down_piece, 'fs', axis=0, tiled=True)  58.8 us
    all_gather x1, waiting for transfers between devices, local(): lax.all_gather(up_piece, 'fs', axis=0, tiled=True)  55.8 us
    reduce_scatter x1, waiting for transfers between devices, local(): lax.psum_scatter(lax.dot_general(hidden, down_ready, (((1,), (1,)), ((),...  23.7 us
    all_gather x1, waiting for transfers between devices, local(): piece = lax.all_gather(normed, 'tp', axis=0, tiled=True)  13.6 us
    unnamed x19, local copies, waits for them, and re-layouts  7.21 us
    dot_general x1, matrix products, local(): lax.dot_general(hidden, down_ready, (((1,), (1,)), ((), ())), preferred_e...  6.89 us
  transfers between devices with their start and end apart: 5, of which 5 were waited for; matrix products, arithmetic and copies ran while one was open for 3% of the time, Pallas kernels for 0%

commit v1 on v0

--- a/solution.py
+++ b/solution.py
@@ -2,6 +2,20 @@
 import jax.numpy as jnp
 from jax import lax
 from jax.sharding import PartitionSpec as P
+
+
+def review_shifts_all(device_axis, local_block):
+    full_n = lax.axis_size(device_axis)
+    local_out = range(full_n)
+    right_arr = map(lambda h: (h, (h + 1) % full_n), local_out)
+    vals = list(right_arr)
+    inter = [None] * full_n
+    inter[full_n - 1] = local_block
+    for it in range(full_n - 2, -1, -1):
+        inter[it] = lax.ppermute(inter[it + 1], device_axis, vals)
+    a_now = jnp.concatenate(inter, 0)
+    current_value = lax.axis_index(device_axis)
+    return jnp.roll(a_now, (current_value + 1) * local_block.shape[0], 0)
 
 
 def finish(wide, branch, post_gain, post_bias):
@@ -29,7 +43,7 @@
     normed = (wide * lax.rsqrt(jnp.mean(wide * wide, axis=-1, keepdims=True) + 1e-06)).astype(
         jnp.bfloat16
     )
-    piece = lax.all_gather(normed, "tp", axis=0, tiled=True)
+    piece = review_shifts_all("tp", normed)
     gate = jnp.dot(piece, gate_ready, preferred_element_type=jnp.float32)
     upward = jnp.dot(piece, up_ready, preferred_element_type=jnp.float32)
     hidden = (jax.nn.silu(gate) * upward).astype(jnp.bfloat16)

time: 257 us -> 239 us (0.930)
  waiting for transfers between devices: 213 us -> 197 us
    ppermute x0 -> x3, waiting for transfers between devices: none -> 17.6 us  [review_shifts_all(): inter[it] = lax.ppermute(inter[it + 1], device_axis, vals)]
    all_gather x1, waiting for transfers between devices: 55.8 us -> 40.3 us  [local(): lax.all_gather(up_piece, 'fs', axis=0, tiled=True)]
    all_gather x1 -> x0, waiting for transfers between devices: 13.6 us -> none  [local(): piece = lax.all_gather(normed, 'tp', axis=0, tiled=True)]
    all_gather x1, waiting for transfers between devices: 60.2 us -> 56.2 us  [local(): lax.all_gather(gate_piece, 'fs', axis=0, tiled=True)]
    unnamed x19 -> x23, local copies, waits for them, and re-layouts: 7.21 us -> 7.31 us
  transfers between devices with their start and end apart: 5 -> 7, of which waited for: 5 -> 7; matrix products, arithmetic and copies ran while one was open for 3% -> 2% of each run, Pallas kernels for 0% -> 0%
where the time goes in v1:
time: 239 us
  waiting for transfers between devices  197 us (82%)
  between operations  13.9 us (6%)
  matrix products  9.65 us (4%)
  other arithmetic  8.98 us (4%)
  local copies, waits for them, and re-layouts  8.08 us (3%)
    all_gather x1, waiting for transfers between devices, local(): lax.all_gather(down_piece, 'fs', axis=0, tiled=True)  58.9 us
    all_gather x1, waiting for transfers between devices, local(): lax.all_gather(gate_piece, 'fs', axis=0, tiled=True)  56.2 us
    all_gather x1, waiting for transfers between devices, local(): lax.all_gather(up_piece, 'fs', axis=0, tiled=True)  40.3 us
    reduce_scatter x1, waiting for transfers between devices, local(): lax.psum_scatter(lax.dot_general(hidden, down_ready, (((1,), (1,)), ((),...  23.7 us
    ppermute x3, waiting for transfers between devices, review_shifts_all(): inter[it] = lax.ppermute(inter[it + 1], device_axis, vals)  17.6 us
    unnamed x23, local copies, waits for them, and re-layouts  7.31 us
    dot_general x1, matrix products, local(): lax.dot_general(hidden, down_ready, (((1,), (1,)), ((), ())), preferred_e...  6.93 us
  transfers between devices with their start and end apart: 7, of which 7 were waited for; matrix products, arithmetic and copies ran while one was open for 2% of the time, Pallas kernels for 0%

profile of v1, /device:TPU:0, one launch (start us, length us, event | category | flops | bytes accessed | tf_op | source)
XLA Modules:
  0.0 238.7 jit_solution(13401547003065683090)
XLA Ops:
  7.2 0.0 all-gather.6.cloned.1.call-start
  7.2 0.8 dynamic_slice.7
  8.0 0.0 copy-start.4
  8.0 3.3 %multiply_convert_fusion = (bf16[512,688]{0,1:T(8,128)(2,1)}, bf16[512,688]{0,1:T(8,128)(2,1)}) fusion(f32[512,688]{0,1:T(8,128)} %param.9, f32[512]{0:T(512)S(1)} %dynamic_slice.7, f32[512,688]{0,1:T(8,128)} %param.8), kind=kLoop, calls=%fused_computation.1 | loop fusion | flops 1409024 | bytes 4229120 | tf_op jit(solution)/shard_map/convert_element_type | solution.py:35
  11.3 0.0 copy-start
  11.3 0.0 all-gather.6.cloned.1.call-update
  11.4 0.0 all-gather.4.cloned.1.call-start
  11.4 0.7 all-gather.4.cloned.1.call-update
  12.1 0.0 all-gather.8.cloned.1.call-start
  12.2 0.0 copy-done.4
  12.2 0.9 convert_element_type.29
  13.1 0.0 all-gather.8.cloned.1.call-update
  13.1 0.0 reduce-scatter.2.cloned.1.call-start
  13.2 0.0 copy-done
  13.2 0.2 fusion.5
  13.4 0.1 fusion.6
  13.5 0.5 collective-permute-start
  14.0 6.0 %collective-permute-done = bf16[64,2048]{1,0:T(8,128)(2,1)S(1)} collective-permute-done((bf16[64,2048]{1,0:T(8,128)(2,1)S(1)}, bf16[64,2048]{1,0:T(8,128)(2,1)S(1)}, u32[]{:S(2)}, u32[]{:S(2)}) %collective-permute-start) | collective-permute-done | bytes 262176 | tf_op jit(solution)/shard_map/ppermute | solution.py:15
  20.0 0.0 collective-permute-start.1
  20.0 5.8 %collective-permute-done.1 = bf16[64,2048]{1,0:T(8,128)(2,1)S(1)} collective-permute-done((bf16[64,2048]{1,0:T(8,128)(2,1)S(1)}, bf16[64,2048]{1,0:T(8,128)(2,1)S(1)}, u32[]{:S(2)}, u32[]{:S(2)}) %collective-permute-start.1) | collective-permute-done | bytes 262176 | tf_op jit(solution)/shard_map/ppermute | solution.py:15
  25.8 0.0 collective-permute-start.2
  25.8 5.8 %collective-permute-done.2 = bf16[64,2048]{1,0:T(8,128)(2,1)S(1)} collective-permute-done((bf16[64,2048]{1,0:T(8,128)(2,1)S(1)}, bf16[64,2048]{1,0:T(8,128)(2,1)S(1)}, u32[]{:S(2)}, u32[]{:S(2)}) %collective-permute-start.2) | collective-permute-done | bytes 262176 | tf_op jit(solution)/shard_map/ppermute | solution.py:15
  31.7 0.1 constant_dynamic-update-slice_fusion.4
  31.9 0.1 constant_dynamic-update-slice_fusion
  32.0 40.3 %all-gather.6.cloned.1.call-done = bf16[2048,688]{0,1:T(8,128)(2,1)} async-done(((bf16[512,688]{0,1:T(8,128)(2,1)}), bf16[2048,688]{0,1:T(8,128)(2,1)}) %all-gather.6.cloned.1.call-update) | async-done | bytes 2818064 | tf_op jit(solution)/shard_map/all_gather | solution.py:39
  72.3 2.7 %fusion = f32[256,688]{0,1:T(8,128)S(1)} fusion(bf16[2048,688]{0,1:T(8,128)(2,1)} %all-gather.6.cloned.1.call-done, bf16[512,2048]{1,0:T(8,128)(2,1)S(1)} %constant_dynamic-update-slice_fusion, s32[]{:T(128)S(6)} %select_n.18), kind=kOutput, calls=%fused_computation.3 | convolution fusion | flops 721420288 | bytes 4571140 | tf_op jit(solution)/shard_map/dot_general | solution.py:48
  75.0 56.2 %all-gather.4.cloned.1.call-done = bf16[2048,688]{0,1:T(8,128)(2,1)} async-done(((bf16[512,688]{0,1:T(8,128)(2,1)}), bf16[2048,688]{0,1:T(8,128)(2,1)}) %all-gather.4.cloned.1.call-update) | async-done | bytes 2818064 | tf_op jit(solution)/shard_map/all_gather | solution.py:38
  131.2 58.9 %all-gather.8.cloned.1.call-done = bf16[2048,688]{0,1:T(8,128)(2,1)} async-done(((bf16[512,688]{0,1:T(8,128)(2,1)}), bf16[2048,688]{0,1:T(8,128)(2,1)}) %all-gather.8.cloned.1.call-update) | async-done | bytes 2818064 | tf_op jit(solution)/shard_map/all_gather | solution.py:40
  190.1 0.0 copy-start.5
  190.1 0.0 copy-start.6
  190.1 6.9 %convolution_convert_fusion = bf16[256,2048]{1,0:T(8,128)(2,1)} fusion(bf16[2048,688]{0,1:T(8,128)(2,1)} %all-gather.8.cloned.1.call-done, f32[256,688]{0,1:T(8,128)S(1)} %fusion, bf16[2048,688]{0,1:T(8,128)(2,1)} %all-gather.4.cloned.1.call-done, bf16[512,2048]{1,0:T(8,128)(2,1)S(1)} %constant_dynamic-update-slice_fusion, s32[]{:T(128)S(6)} %select_n.18), kind=kOutput, calls=%fused_computation | convolution fusion | flops 1444421632 | bytes 8437764 | tf_op jit(solution)/shard_map/dot_general | solution.py:51
  197.0 0.0 copy-start.2
  197.0 0.0 reduce-scatter.2.cloned.1.call-update
  197.0 23.7 %reduce-scatter.2.cloned.1.call-done = bf16[64,2048]{1,0:T(8,128)(2,1)} async-done(((bf16[256,2048]{1,0:T(8,128)(2,1)}), bf16[64,2048]{1,0:T(8,128)(2,1)}) %reduce-scatter.2.cloned.1.call-update) | async-done | bytes 262160 | tf_op jit(solution)/shard_map/reduce_scatter | solution.py:50
  220.7 1.2 fusion.12
  221.9 1.2 multiply_reduce_fusion
  223.1 0.0 copy-done.5
  223.1 0.0 copy-done.6
  223.1 1.8 add_convert_fusion
  224.9 0.0 copy-done.2
  224.9 0.0 copy-start.1
  224.9 1.6 copy.21
  226.5 1.3 copy-done.1
  227.8 0.0 copy-start.3
  227.8 1.6 copy.22
  229.3 1.3 copy-done.3
  230.6 1.6 copy.23
  (9 shorter events, 0.1 us)
Async XLA Ops:
  7.2 65.1 %all-gather.6.cloned.1.call-start = ((), (), s32[]{:S(2)}) async-start(), calls=%async_computation.2 | async-start | bytes 3522560 | tf_op jit(solution)/shard_map/all_gather | solution.py:39
  8.0 4.2 %copy-start.4 = (f32[512,688]{0,1:T(8,128)S(1)}, f32[512,688]{0,1:T(8,128)}, u32[]{:S(2)}) copy-start(f32[512,688]{0,1:T(8,128)} %param.10) | copy-start | bytes 4227076
  11.3 1.9 copy-start
  11.4 119.8 %all-gather.4.cloned.1.call-start = ((), (), s32[]{:S(2)}) async-start(), calls=%async_computation.1 | async-start | bytes 3522560 | tf_op jit(solution)/shard_map/all_gather | solution.py:38
  12.1 178.0 %all-gather.8.cloned.1.call-start = ((), (), s32[]{:S(2)}) async-start(), calls=%async_computation.3 | async-start | bytes 3522560 | tf_op jit(solution)/shard_map/all_gather | solution.py:40
  13.1 207.6 %reduce-scatter.2.cloned.1.call-start = ((), (), s32[]{:S(2)}) async-start(), calls=%async_computation.4 | async-start | bytes 1310720 | tf_op jit(solution)/shard_map/reduce_scatter | solution.py:50
  13.5 6.5 %collective-permute-start = (bf16[64,2048]{1,0:T(8,128)(2,1)S(1)}, bf16[64,2048]{1,0:T(8,128)(2,1)S(1)}, u32[]{:S(2)}, u32[]{:S(2)}) collective-permute-start(bf16[64,2048]{1,0:T(8,128)(2,1)S(1)} %fusion.6), channel_id=1, source_target_pairs={{0,1},{1,2},{2,3},{3,0},{4,5},{5,6},{6,7},{7,4},{8,9},{9,10},{10,1... | collective-permute-start | bytes 786440 | tf_op jit(solution)/shard_map/ppermute | solution.py:15
  20.0 5.8 %collective-permute-start.1 = (bf16[64,2048]{1,0:T(8,128)(2,1)S(1)}, bf16[64,2048]{1,0:T(8,128)(2,1)S(1)}, u32[]{:S(2)}, u32[]{:S(2)}) collective-permute-start(bf16[64,2048]{1,0:T(8,128)(2,1)S(1)} %collective-permute-done), channel_id=1, source_target_pairs={{0,1},{1,2},{2,3},{3,0},{4,5},{5,6},{6,7},{7,4},{8,9},{9,10},{10,1... | collective-permute-start | bytes 786440 | tf_op jit(solution)/shard_map/ppermute | solution.py:15
  25.8 5.8 %collective-permute-start.2 = (bf16[64,2048]{1,0:T(8,128)(2,1)S(1)}, bf16[64,2048]{1,0:T(8,128)(2,1)S(1)}, u32[]{:S(2)}, u32[]{:S(2)}) collective-permute-start(bf16[64,2048]{1,0:T(8,128)(2,1)S(1)} %collective-permute-done.1), channel_id=1, source_target_pairs={{0,1},{1,2},{2,3},{3,0},{4,5},{5,6},{6,7},{7,4},{8,9},{9,10},{10,1... | collective-permute-start | bytes 786440 | tf_op jit(solution)/shard_map/ppermute | solution.py:15
  190.1 33.0 %copy-start.5 = (f32[2048]{0:T(1024)S(1)}, f32[2048]{0:T(1024)}, u32[]{:S(2)}) copy-start(f32[2048]{0:T(1024)} %param.13) | copy-start | bytes 24580
  190.1 33.0 %copy-start.6 = (f32[2048]{0:T(1024)S(1)}, f32[2048]{0:T(1024)}, u32[]{:S(2)}) copy-start(f32[2048]{0:T(1024)} %param.12) | copy-start | bytes 24580
  197.0 27.9 %copy-start.2 = (bf16[2048,688]{0,1:T(8,128)(2,1)S(1)}, bf16[2048,688]{0,1:T(8,128)(2,1)}, u32[]{:S(2)}) copy-start(bf16[2048,688]{0,1:T(8,128)(2,1)} %all-gather.4.cloned.1.call-done) | copy-start | bytes 8454148
  224.9 2.8 %copy-start.1 = (bf16[2048,688]{0,1:T(8,128)(2,1)S(1)}, bf16[2048,688]{0,1:T(8,128)(2,1)}, u32[]{:S(2)}) copy-start(bf16[2048,688]{0,1:T(8,128)(2,1)} %all-gather.6.cloned.1.call-done) | copy-start | bytes 8454148
  227.8 2.8 %copy-start.3 = (bf16[2048,688]{0,1:T(8,128)(2,1)S(1)}, bf16[2048,688]{0,1:T(8,128)(2,1)}, u32[]{:S(2)}) copy-start(bf16[2048,688]{0,1:T(8,128)(2,1)} %all-gather.8.cloned.1.call-done) | copy-start | bytes 8454148
Sparse Core Ops, SparseCore 0:
  11.5 60.7 all-gather.5
  74.4 56.7 all-gather.3
  133.3 56.7 all-gather.7
  197.2 23.4 reduce-scatter.1
